TPU v7x, 32 devices: a whole 2x2x4 slice. The times are simulated.
32 devices in a mesh: grp: 2 (over y), sp: 4 (over z), tp: 4 (over x, core).
Axes of the slice: x: 2, y: 2, z: 4, core: 2. Of those that a mesh axis runs over, the one named last changes fastest.
Arguments:
- source: bfloat16 [4096, 2048], P(('grp', 'sp', 'tp')), parts along dimension 0, may hold values from -8 to 8
- target: bfloat16 [1024, 2048], P(('grp', 'sp', 'tp')), parts along dimension 0, may hold values from -8 to 8
- source_gain: float32 [2048], replicated, may hold values from 0.1 to 1.9
- attend_gain: float32 [2, 2048], replicated, may hold values from 0.1 to 1.9
- query_weight: bfloat16 [2, 2048, 2048], P(None, None, 'tp'), may hold values from -4 to 4
- key_weight: bfloat16 [2, 2048, 2048], P(None, None, 'tp'), may hold values from -4 to 4
- value_weight: bfloat16 [2, 2048, 2048], P(None, None, 'tp'), may hold values from -0.125 to 0.125
- out_weight: bfloat16 [2, 2048, 2048], P(None, 'tp'), may hold values from -3 to 3
- mixer_gain: float32 [2048], replicated, may hold values from 0.1 to 1.9
- gate_weight: bfloat16 [2048, 2816], P(None, 'tp'), may hold values from -0.125 to 0.125
- up_weight: bfloat16 [2048, 2816], P(None, 'tp'), may hold values from -0.125 to 0.125
- gate_taps: float32 [3, 2816], P(None, 'tp'), may hold values from -3 to 3
- up_taps: float32 [3, 2816], P(None, 'tp'), may hold values from -3 to 3
- down_weight: bfloat16 [2816, 2048], P('tp'), may hold values from -0.109375 to 0.109375
- final_gain: float32 [2048], replicated, may hold values from 0.1 to 1.9
Outputs:
- result: bfloat16 [1024, 2048], P(('grp', 'sp', 'tp')), parts along dimension 0
There are 2 independent parts, one for each index of `grp`. A program takes and returns all parts, laid end to end along the dimension named above; an argument that names none is the same for every part. Nothing has to cross between parts.
All inputs are finite; a program needn't handle non-finite values.
Results may differ from a plain program's by a relative error of at most 0.04.
Values may be sent and summed in bfloat16 or wider, within the bound.
A program may use at most 128 MiB of HBM per device.

v0:
```python
import jax
import jax.numpy as jnp
from jax import lax
from jax.sharding import PartitionSpec as P

HD = 256
EPS = 1e-06


def shifted(value, axis, steps):
    count = lax.axis_size(axis)
    first, last = (max(0, -steps), min(count, count - steps))
    return lax.ppermute(value, axis, [(source, source + steps) for source in range(first, last)])


def normed_rows(rows, gain):
    wide = rows.astype(jnp.float32)
    return wide * lax.rsqrt(jnp.mean(wide * wide, axis=-1, keepdims=True) + EPS) * gain


def attend_layer(residual, key_rows, value_rows, gain, w_query, w_out):
    width = w_query.shape[1]
    heads_here = width // HD
    head_scale = HD ** (-0.5)
    normed = normed_rows(residual, gain).astype(jnp.bfloat16)
    query_block = jnp.dot(
        lax.all_gather(normed, "tp", axis=0, tiled=True),
        w_query,
        preferred_element_type=jnp.float32,
    ).astype(jnp.bfloat16)
    row_count = query_block.shape[0]
    key_heads = key_rows.reshape(-1, heads_here, HD)
    value_heads = value_rows.reshape(-1, heads_here, HD)
    every_query = lax.all_gather(query_block, "sp", axis=0, tiled=True)
    every_heads = every_query.reshape(-1, heads_here, HD)
    scores = (
        jnp.einsum("thd,shd->hts", every_heads, key_heads, preferred_element_type=jnp.float32)
        * head_scale
    )
    highest = lax.pmax(jnp.max(scores, axis=-1), "sp")
    raised = jnp.exp(scores - highest[:, :, None])
    weighted = jnp.einsum(
        "hts,shd->thd", raised.astype(jnp.bfloat16), value_heads, preferred_element_type=jnp.float32
    )
    row_totals = jnp.sum(raised, axis=-1).T
    own_sums, own_totals = (
        lax.psum_scatter(
            weighted.astype(jnp.bfloat16), "sp", scatter_dimension=0, tiled=True
        ).astype(jnp.float32),
        lax.psum_scatter(
            row_totals.astype(jnp.bfloat16), "sp", scatter_dimension=0, tiled=True
        ).astype(jnp.float32),
    )
    attended = (own_sums / own_totals[:, :, None]).reshape(row_count, width).astype(jnp.bfloat16)
    return lax.psum_scatter(
        jnp.dot(attended, w_out, preferred_element_type=jnp.float32).astype(jnp.bfloat16),
        "tp",
        scatter_dimension=0,
        tiled=True,
    ).astype(jnp.float32)


def body(
    source,
    target,
    source_gain,
    attend_gain,
    query_weight,
    key_weight,
    value_weight,
    out_weight,
    mixer_gain,
    gate_weight,
    up_weight,
    gate_taps,
    up_taps,
    down_weight,
    final_gain,
):
    width = query_weight.shape[2]
    source_normed = normed_rows(source, source_gain).astype(jnp.bfloat16)
    joined_weights = jnp.concatenate(
        [key_weight[0], value_weight[0], key_weight[1], value_weight[1]], axis=1
    )
    projected = jnp.dot(
        lax.all_gather(source_normed, "tp", axis=0, tiled=True),
        joined_weights,
        preferred_element_type=jnp.float32,
    ).astype(jnp.bfloat16)
    residual = target.astype(jnp.float32)
    for layer_number in range(2):
        key_rows = projected[:, 2 * layer_number * width : (2 * layer_number + 1) * width]
        value_rows = projected[:, (2 * layer_number + 1) * width : (2 * layer_number + 2) * width]
        residual = residual + attend_layer(
            residual,
            key_rows,
            value_rows,
            attend_gain[layer_number],
            query_weight[layer_number],
            out_weight[layer_number],
        )
    mixed = normed_rows(residual, mixer_gain).astype(jnp.bfloat16)
    portion = lax.all_gather(mixed, "tp", axis=0, tiled=True)
    gate_part = jnp.dot(portion, gate_weight, preferred_element_type=jnp.float32)
    up_part = jnp.dot(portion, up_weight, preferred_element_type=jnp.float32)
    lifted = jnp.concatenate([gate_part, up_part], axis=1).astype(jnp.bfloat16)
    earlier = shifted(lifted[-2:], "sp", 1)
    padded = jnp.concatenate([earlier, lifted], axis=0).astype(jnp.float32)
    all_taps = jnp.concatenate([gate_taps, up_taps], axis=1)
    convolved = all_taps[0] * padded[:-2] + all_taps[1] * padded[1:-1] + all_taps[2] * padded[2:]
    inner_units = gate_weight.shape[1]
    hidden = (jax.nn.silu(convolved[:, :inner_units]) * convolved[:, inner_units:]).astype(
        jnp.bfloat16
    )
    residual = residual + lax.psum_scatter(
        jnp.dot(hidden, down_weight, preferred_element_type=jnp.float32).astype(jnp.bfloat16),
        "tp",
        scatter_dimension=0,
        tiled=True,
    ).astype(jnp.float32)
    return normed_rows(residual, final_gain).astype(jnp.bfloat16)


def solution(mesh):
    placed = (
        P(("grp", "sp", "tp"), None),
        P(("grp", "sp", "tp"), None),
        P(),
        P(),
        P(None, None, "tp"),
        P(None, None, "tp"),
        P(None, None, "tp"),
        P(None, "tp", None),
        P(),
        P(None, "tp"),
        P(None, "tp"),
        P(None, "tp"),
        P(None, "tp"),
        P("tp", None),
        P(),
    )
    return jax.shard_map(
        body, mesh=mesh, in_specs=placed, out_specs=P(("grp", "sp", "tp"), None), check_vma=False
    )
```

profile of v0, /device:TPU:0, one launch (start us, length us, event | category | flops | bytes accessed | tf_op | source)
XLA Modules:
  0.0 301.9 jit_solution(114304977294703288)
XLA Ops:
  10.4 8.8 %all_gather.19 = bf16[128,2048]{1,0:T(8,128)(2,1)S(1)} all-gather(bf16[32,2048]{1,0:T(8,128)(2,1)S(1)} %fusion.55), channel_id=1, replica_groups=mesh['grp'=2,'sp'=4,'tp'=4] {'tp'}, dimensions={0}, use_global_device_ids=true | all-gather | bytes 655360 | tf_op jit(solution)/shard_map/all_gather | solution.py:27
  19.2 2.2 fusion.25
  21.3 16.3 %all_gather.20 = bf16[512,512]{1,0:T(8,128)(2,1)S(1)} all-gather(bf16[128,512]{1,0:T(8,128)(2,1)S(1)} %fusion.25), channel_id=1, replica_groups=mesh['grp'=2,'sp'=4,'tp'=4] {'sp'}, dimensions={0}, use_global_device_ids=true | all-gather | bytes 655360 | tf_op jit(solution)/shard_map/all_gather | solution.py:34
  37.7 4.9 %slice_bitcast_fusion.2 = (bf16[2048,512]{1,0:T(8,128)(2,1)}, bf16[2048,512]{1,0:T(8,128)(2,1)}, bf16[2048,512]{1,0:T(8,128)(2,1)}, bf16[2048,512]{1,0:T(8,128)(2,1)}) fusion(bf16[2,2048,512]{2,1,0:T(8,128)(2,1)S(1)} %copy-done.3, bf16[2,2048,512]{2,1,0:T(8,128)(2,1)} %param.20), kind=kLoop, calls=%fused_computation.26 | loop fusion | bytes 16777216 | tf_op jit(solution)/shard_map/squeeze | solution.py:83
  42.6 8.9 %fusion.8 = bf16[512,2048]{1,0:T(8,128)(2,1)S(1)} fusion(bf16[512,2048]{1,0:T(8,128)(2,1)} %all-gather.2.cloned.1.call-done, bf16[2048,512]{1,0:T(8,128)(2,1)} %get-tuple-element.11, bf16[2048,512]{1,0:T(8,128)(2,1)} %get-tuple-element.22, bf16[2048,512]{1,0:T(8,128)(2,1)} %get-tuple-element.10, bf16[2048,512]{1,0:T(8,128)(2,1)} %get-tuple-element.23), kind=kOutput, calls=%fused_computation.8 | convolution fusion | flops 4329570304 | bytes 12582912 | tf_op jit(solution)/shard_map/dot_general | solution.py:85
  54.5 12.1 %pmax.14 = f32[2,512]{1,0:T(2,128)S(1)} all-reduce(f32[2,512]{1,0:T(2,128)S(1)} %get-tuple-element.18), channel_id=1, replica_groups=mesh['grp'=2,'sp'=4,'tp'=4] {'sp'}, use_global_device_ids=true, to_apply=%region_3.0 | all-reduce | flops 1024 | bytes 8192 | tf_op jit(solution)/shard_map/pmax | solution.py:40
  70.7 2.9 convolution_convert_fusion.4
  75.8 12.4 %reduce-scatter.24.cloned.1.call-done = bf16[128,2]{1,0:T(8,128)(2,1)} async-done(((bf16[512,2]{1,0:T(8,128)(2,1)}), bf16[128,2]{1,0:T(8,128)(2,1)}) %reduce-scatter.24.cloned.1.call-update) | async-done | bytes 528
  89.0 21.5 %reduce-scatter.22.cloned.1.call-done = bf16[128,512]{1,0:T(8,128)(2,1)} async-done(((bf16[512,512]{1,0:T(8,128)(2,1)}), bf16[128,512]{1,0:T(8,128)(2,1)}) %reduce-scatter.22.cloned.1.call-update) | async-done | bytes 131088
  111.5 2.9 convolution_convert_fusion.2
  115.7 18.8 %reduce-scatter.16.cloned.1.call-done = bf16[32,2048]{1,0:T(8,128)(2,1)} async-done(((bf16[128,2048]{1,0:T(8,128)(2,1)}), bf16[32,2048]{1,0:T(8,128)(2,1)}) %reduce-scatter.16.cloned.1.call-update) | async-done | bytes 131088 | tf_op jit(solution)/shard_map/reduce_scatter | solution.py:55
  136.5 6.6 %all_gather.21 = bf16[128,2048]{1,0:T(8,128)(2,1)S(1)} all-gather(bf16[32,2048]{1,0:T(8,128)(2,1)S(1)} %multiply_convert_fusion.2), channel_id=1, replica_groups=mesh['grp'=2,'sp'=4,'tp'=4] {'tp'}, dimensions={0}, use_global_device_ids=true | all-gather | bytes 655360 | tf_op jit(solution)/shard_map/all_gather | solution.py:27
  145.2 16.1 %all_gather.22 = bf16[512,512]{1,0:T(8,128)(2,1)S(1)} all-gather(bf16[128,512]{1,0:T(8,128)(2,1)S(1)} %fusion.28), channel_id=1, replica_groups=mesh['grp'=2,'sp'=4,'tp'=4] {'sp'}, dimensions={0}, use_global_device_ids=true | all-gather | bytes 655360 | tf_op jit(solution)/shard_map/all_gather | solution.py:34
  163.1 12.2 %pmax.15 = f32[2,512]{1,0:T(2,128)S(1)} all-reduce(f32[2,512]{1,0:T(2,128)S(1)} %get-tuple-element.20), channel_id=1, replica_groups=mesh['grp'=2,'sp'=4,'tp'=4] {'sp'}, use_global_device_ids=true, to_apply=%region_10.0 | all-reduce | flops 1024 | bytes 8192 | tf_op jit(solution)/shard_map/pmax | solution.py:40
  178.2 2.9 convolution_convert_fusion.3
  183.2 12.2 %reduce-scatter.28.cloned.1.call-done = bf16[128,2]{1,0:T(8,128)(2,1)} async-done(((bf16[512,2]{1,0:T(8,128)(2,1)}), bf16[128,2]{1,0:T(8,128)(2,1)}) %reduce-scatter.28.cloned.1.call-update) | async-done | bytes 528
  196.3 21.4 %reduce-scatter.26.cloned.1.call-done = bf16[128,512]{1,0:T(8,128)(2,1)} async-done(((bf16[512,512]{1,0:T(8,128)(2,1)}), bf16[128,512]{1,0:T(8,128)(2,1)}) %reduce-scatter.26.cloned.1.call-update) | async-done | bytes 131088
  218.7 2.9 convolution_convert_fusion.1
  221.6 20.0 %reduce-scatter.18.cloned.1.call-done = bf16[32,2048]{1,0:T(8,128)(2,1)} async-done(((bf16[128,2048]{1,0:T(8,128)(2,1)}), bf16[32,2048]{1,0:T(8,128)(2,1)}) %reduce-scatter.18.cloned.1.call-update) | async-done | bytes 131088 | tf_op jit(solution)/shard_map/reduce_scatter | solution.py:55
  243.7 6.9 %all_gather.23 = bf16[128,2048]{1,0:T(8,128)(2,1)S(1)} all-gather(bf16[32,2048]{1,0:T(8,128)(2,1)S(1)} %multiply_convert_fusion.1), channel_id=1, replica_groups=mesh['grp'=2,'sp'=4,'tp'=4] {'tp'}, dimensions={0}, use_global_device_ids=true | all-gather | bytes 655360 | tf_op jit(solution)/shard_map/all_gather | solution.py:103
  250.6 2.7 convolution_convert_fusion.5
  254.5 3.4 %collective-permute-start = (bf16[2,1408]{0,1:T(8,128)(2,1)S(1)}, bf16[2,1408]{0,1:T(8,128)(2,1)S(1)}, u32[]{:S(2)}, u32[]{:S(2)}) collective-permute-start(bf16[2,1408]{0,1:T(8,128)(2,1)S(1)} %pad_maximum_fusion), channel_id=1, source_target_pairs={{0,4},{4,8},{8,12},{1,5},{5,9},{9,13},{2,6},{6,10},{10,14},{3,7},{... | collective-permute-start | bytes 16904 | tf_op jit(solution)/shard_map/ppermute | solution.py:13
  258.0 8.0 %collective-permute-done = bf16[2,1408]{0,1:T(8,128)(2,1)S(1)} collective-permute-done((bf16[2,1408]{0,1:T(8,128)(2,1)S(1)}, bf16[2,1408]{0,1:T(8,128)(2,1)S(1)}, u32[]{:S(2)}, u32[]{:S(2)}) %collective-permute-start) | collective-permute-done | bytes 5664 | tf_op jit(solution)/shard_map/ppermute | solution.py:13
  269.0 23.3 %reduce-scatter.20.cloned.1.call-done = bf16[32,2048]{1,0:T(8,128)(2,1)} async-done(((bf16[128,2048]{1,0:T(8,128)(2,1)}), bf16[32,2048]{1,0:T(8,128)(2,1)}) %reduce-scatter.20.cloned.1.call-update) | async-done | bytes 131088 | tf_op jit(solution)/shard_map/reduce_scatter | solution.py:115
  (83 shorter events, 38.0 us)
Async XLA Ops:
  6.5 261.0 %copy-start = (bf16[704,2048]{1,0:T(8,128)(2,1)S(1)}, bf16[704,2048]{1,0:T(8,128)(2,1)}, u32[]{:S(2)}) copy-start(bf16[704,2048]{1,0:T(8,128)(2,1)} %param.28) | copy-start | bytes 8650756
  6.5 3.5 %copy-start.1 = (bf16[32,2048]{1,0:T(8,128)(2,1)S(1)}, bf16[32,2048]{1,0:T(8,128)(2,1)}, u32[]{:S(2)}) copy-start(bf16[32,2048]{1,0:T(8,128)(2,1)} %param.16) | copy-start | bytes 393220
  6.5 3.7 %copy-start.7 = (f32[2,2048]{1,0:T(2,128)S(1)}, f32[2,2048]{1,0:T(2,128)}, u32[]{:S(2)}) copy-start(f32[2,2048]{1,0:T(2,128)} %param.18) | copy-start | bytes 49156
  6.5 36.1 %all-gather.2.cloned.1.call-start = ((), (), s32[]{:S(2)}) async-start(), calls=%async_computation.7 | async-start | bytes 2621440 | tf_op jit(solution)/shard_map/all_gather | solution.py:86
  10.0 78.1 %reduce-scatter.24.cloned.1.call-start = ((), (), s32[]{:S(2)}) async-start(), calls=%async_computation.12 | async-start | bytes 163840
  10.4 27.3 %copy-start.3 = (bf16[2,2048,512]{2,1,0:T(8,128)(2,1)S(1)}, bf16[2,2048,512]{2,1,0:T(8,128)(2,1)}, u32[]{:S(2)}) copy-start(bf16[2,2048,512]{2,1,0:T(8,128)(2,1)} %param.21) | copy-start | bytes 12582916
  70.7 39.7 %reduce-scatter.22.cloned.1.call-start = ((), (), s32[]{:S(2)}) async-start(), calls=%async_computation.11 | async-start | bytes 655360
  75.7 58.7 %reduce-scatter.16.cloned.1.call-start = ((), (), s32[]{:S(2)}) async-start(), calls=%async_computation.8 | async-start | bytes 655360 | tf_op jit(solution)/shard_map/reduce_scatter | solution.py:55
  114.4 81.1 %reduce-scatter.28.cloned.1.call-start = ((), (), s32[]{:S(2)}) async-start(), calls=%async_computation.14 | async-start | bytes 163840
  143.1 18.2 %copy-start.6 = (bf16[512,512]{1,0:T(8,128)(2,1)S(1)}, bf16[512,512]{1,0:T(8,128)(2,1)}, u32[]{:S(2)}) copy-start(bf16[512,512]{1,0:T(8,128)(2,1)} %get-tuple-element.13) | copy-start | bytes 1572868
  178.1 39.5 %reduce-scatter.26.cloned.1.call-start = ((), (), s32[]{:S(2)}) async-start(), calls=%async_computation.13 | async-start | bytes 655360
  183.1 58.5 %copy-start.2 = (bf16[32,2048]{1,0:T(8,128)(2,1)S(1)}, bf16[32,2048]{1,0:T(8,128)(2,1)}, u32[]{:S(2)}) copy-start(bf16[32,2048]{1,0:T(8,128)(2,1)} %reduce-scatter.16.cloned.1.call-done) | copy-start | bytes 393220
  183.2 58.4 %reduce-scatter.18.cloned.1.call-start = ((), (), s32[]{:S(2)}) async-start(), calls=%async_computation.9 | async-start | bytes 655360 | tf_op jit(solution)/shard_map/reduce_scatter | solution.py:55
  196.3 46.4 %copy-start.10 = (f32[2048]{0:T(1024)S(1)}, f32[2048]{0:T(1024)}, u32[]{:S(2)}) copy-start(f32[2048]{0:T(1024)} %param.23) | copy-start | bytes 24580
  221.6 70.7 %reduce-scatter.20.cloned.1.call-start = ((), (), s32[]{:S(2)}) async-start(), calls=%async_computation.10 | async-start | bytes 655360 | tf_op jit(solution)/shard_map/reduce_scatter | solution.py:115
  243.7 9.7 %copy-start.4 = (bf16[2048,704]{0,1:T(8,128)(2,1)S(1)}, bf16[2048,704]{0,1:T(8,128)(2,1)}, u32[]{:S(2)}) copy-start(bf16[2048,704]{0,1:T(8,128)(2,1)} %param.24) | copy-start | bytes 8650756
  253.4 4.5 %copy-start.8 = (f32[3,704]{1,0:T(4,128)S(1)}, f32[3,704]{1,0:T(4,128)}, u32[]{:S(2)}) copy-start(f32[3,704]{1,0:T(4,128)} %param.27) | copy-start | bytes 25348
  253.4 4.5 %copy-start.9 = (f32[3,704]{1,0:T(4,128)S(1)}, f32[3,704]{1,0:T(4,128)}, u32[]{:S(2)}) copy-start(f32[3,704]{1,0:T(4,128)} %param.26) | copy-start | bytes 25348
  254.5 11.6 %collective-permute-start = (bf16[2,1408]{0,1:T(8,128)(2,1)S(1)}, bf16[2,1408]{0,1:T(8,128)(2,1)S(1)}, u32[]{:S(2)}, u32[]{:S(2)}) collective-permute-start(bf16[2,1408]{0,1:T(8,128)(2,1)S(1)} %pad_maximum_fusion), channel_id=1, source_target_pairs={{0,4},{4,8},{8,12},{1,5},{5,9},{9,13},{2,6},{6,10},{10,14},{3,7},{... | collective-permute-start | bytes 16904 | tf_op jit(solution)/shard_map/ppermute | solution.py:13
  267.5 24.8 %copy-start.5 = (bf16[32,2048]{1,0:T(8,128)(2,1)S(1)}, bf16[32,2048]{1,0:T(8,128)(2,1)}, u32[]{:S(2)}) copy-start(bf16[32,2048]{1,0:T(8,128)(2,1)} %reduce-scatter.18.cloned.1.call-done) | copy-start | bytes 393220
  267.5 25.9 %copy-start.11 = (f32[2048]{0:T(1024)S(1)}, f32[2048]{0:T(1024)}, u32[]{:S(2)}) copy-start(f32[2048]{0:T(1024)} %param.29) | copy-start | bytes 24580
Sparse Core Ops, SparseCore 0:
  10.1 25.2 all-gather.1
  70.8 17.2 reduce-scatter.23
  90.4 19.9 reduce-scatter.21
  114.5 19.9 reduce-scatter.15
  178.2 17.1 reduce-scatter.27
  197.6 20.0 reduce-scatter.25
  221.7 19.8 reduce-scatter.17
  269.1 23.1 reduce-scatter.19
where the time goes:
time: 303 us; the launch traced here: 302 us
  waiting for transfers between devices  138 us (46%)
  blocking collectives  79 us (26%)
  matrix products  33.5 us (11%)
  local copies, waits for them, and re-layouts  18.1 us (6%)
  other arithmetic  16.3 us (5%)
  between operations  13.8 us (5%)
  starting transfers between devices  3.69 us (1%)
    unnamed x12, waiting for transfers between devices  67.5 us
    reduce_scatter x2, waiting for transfers between devices, attend_layer(): lax.psum_scatter(jnp.dot(attended, w_out, preferred_element_type=jnp.floa...  38.7 us
    all_gather x2, blocking collectives, attend_layer(): every_query = lax.all_gather(query_block, 'sp', axis=0, tiled=True)  32.4 us
    pmax x2, blocking collectives, attend_layer(): highest = lax.pmax(jnp.max(scores, axis=-1), 'sp')  24.3 us
    reduce_scatter x1, waiting for transfers between devices, body(): lax.psum_scatter(jnp.dot(hidden, down_weight, preferred_element_type=jnp....  23.3 us
    all_gather x2, blocking collectives, attend_layer(): lax.all_gather(normed, 'tp', axis=0, tiled=True)  15.4 us
    unnamed x32, local copies, waits for them, and re-layouts  9.48 us
    dot_general x1, matrix products, body(): jnp.dot(lax.all_gather(source_normed, 'tp', axis=0, tiled=True), joined_w...  8.9 us
  transfers between devices with their start and end apart: 9, of which 8 were waited for; matrix products, arithmetic and copies ran while one was open for 7% of the time, Pallas kernels for 0%

commit v1 on v0

--- a/solution.py
+++ b/solution.py
@@ -31,7 +31,12 @@
     row_count = query_block.shape[0]
     key_heads = key_rows.reshape(-1, heads_here, HD)
     value_heads = value_rows.reshape(-1, heads_here, HD)
-    every_query = lax.all_gather(query_block, "sp", axis=0, tiled=True)
+    ring = [query_block]
+    for hop in range(3):
+        ring.append(lax.ppermute(ring[-1], "sp", [(dev, (dev + 1) % 4) for dev in range(4)]))
+    every_query = jnp.roll(
+        jnp.concatenate(ring[::-1], axis=0), (lax.axis_index("sp") + 1) * ring[0].shape[0], axis=0
+    )
     every_heads = every_query.reshape(-1, heads_here, HD)
     scores = (
         jnp.einsum("thd,shd->hts", every_heads, key_heads, preferred_element_type=jnp.float32)

time: 303 us -> 316 us (1.043)
  blocking collectives: 79 us -> 40.8 us
  waiting for transfers between devices: 138 us -> 174 us
  local copies, waits for them, and re-layouts: 18.1 us -> 23.5 us
  other arithmetic: 16.3 us -> 20.8 us
    ppermute x0 -> x6, waiting for transfers between devices: none -> 33.6 us  [attend_layer(): lax.ppermute(ring[-1], 'sp', [(dev, (dev + 1) % 4) for dev in range(4)])]
    all_gather x2 -> x0, blocking collectives: 32.4 us -> none  [attend_layer(): every_query = lax.all_gather(query_block, 'sp', axis=0, tiled=True)]
    pmax x2, blocking collectives: 24.3 us -> 18.7 us  [attend_layer(): highest = lax.pmax(jnp.max(scores, axis=-1), 'sp')]
    concatenate x0 -> x2, other arithmetic: none -> 4.46 us  [attend_layer(): jnp.roll(jnp.concatenate(ring[::-1], axis=0), (lax.axis_index('sp') + 1)...]
    unnamed x32 -> x48, local copies, waits for them, and re-layouts: 9.48 us -> 12.1 us
  transfers between devices with their start and end apart: 9 -> 15, of which waited for: 8 -> 14; matrix products, arithmetic and copies ran while one was open for 7% -> 7% of each run, Pallas kernels for 0% -> 0%
where the time goes in v1:
time: 316 us; the launch traced here: 315 us
  waiting for transfers between devices  174 us (55%)
  blocking collectives  40.8 us (13%)
  matrix products  35.6 us (11%)
  local copies, waits for them, and re-layouts  23.5 us (7%)
  other arithmetic  20.8 us (7%)
  between operations  13.8 us (4%)
  starting transfers between devices  6.82 us (2%)
    unnamed x12, waiting for transfers between devices  69.1 us
    reduce_scatter x2, waiting for transfers between devices, attend_layer(): lax.psum_scatter(jnp.dot(attended, w_out, preferred_element_type=jnp.floa...  40 us
    ppermute x6, waiting for transfers between devices, attend_layer(): lax.ppermute(ring[-1], 'sp', [(dev, (dev + 1) % 4) for dev in range(4)])  33.6 us
    reduce_scatter x1, waiting for transfers between devices, body(): lax.psum_scatter(jnp.dot(hidden, down_weight, preferred_element_type=jnp....  23.4 us
    pmax x2, blocking collectives, attend_layer(): highest = lax.pmax(jnp.max(scores, axis=-1), 'sp')  18.7 us
    all_gather x2, blocking collectives, attend_layer(): lax.all_gather(normed, 'tp', axis=0, tiled=True)  15.4 us
    unnamed x48, local copies, waits for them, and re-layouts  12.1 us
    dot_general x1, matrix products, body(): jnp.dot(lax.all_gather(source_normed, 'tp', axis=0, tiled=True), joined_w...  8.86 us
  transfers between devices with their start and end apart: 15, of which 14 were waited for; matrix products, arithmetic and copies ran while one was open for 7% of the time, Pallas kernels for 0%

profile of v1, /device:TPU:0, one launch (start us, length us, event | category | flops | bytes accessed | tf_op | source)
XLA Modules:
  0.0 315.4 jit_solution(6345947291347882894)
XLA Ops:
  10.4 8.8 %all_gather.13 = bf16[128,2048]{1,0:T(8,128)(2,1)S(1)} all-gather(bf16[32,2048]{1,0:T(8,128)(2,1)S(1)} %fusion.65), channel_id=1, replica_groups=mesh['grp'=2,'sp'=4,'tp'=4] {'tp'}, dimensions={0}, use_global_device_ids=true | all-gather | bytes 655360 | tf_op jit(solution)/shard_map/all_gather | solution.py:27
  23.6 6.0 %collective-permute-done = bf16[128,512]{1,0:T(8,128)(2,1)S(1)} collective-permute-done((bf16[128,512]{1,0:T(8,128)(2,1)S(1)}, bf16[128,512]{1,0:T(8,128)(2,1)S(1)}, u32[]{:S(2)}, u32[]{:S(2)}) %collective-permute-start) | collective-permute-done | bytes 131104 | tf_op jit(solution)/shard_map/ppermute | solution.py:36
  30.2 6.8 %collective-permute-done.1 = bf16[128,512]{1,0:T(8,128)(2,1)S(1)} collective-permute-done((bf16[128,512]{1,0:T(8,128)(2,1)S(1)}, bf16[128,512]{1,0:T(8,128)(2,1)S(1)}, u32[]{:S(2)}, u32[]{:S(2)}) %collective-permute-start.1) | collective-permute-done | bytes 131104 | tf_op jit(solution)/shard_map/ppermute | solution.py:36
  37.0 5.0 %slice_bitcast_fusion.2 = (bf16[2048,512]{1,0:T(8,128)(2,1)}, bf16[2048,512]{1,0:T(8,128)(2,1)}, bf16[2048,512]{1,0:T(8,128)(2,1)}, bf16[2048,512]{1,0:T(8,128)(2,1)}) fusion(bf16[2,2048,512]{2,1,0:T(8,128)(2,1)S(1)} %copy-done.3, bf16[2,2048,512]{2,1,0:T(8,128)(2,1)} %param.22), kind=kLoop, calls=%fused_computation.26 | loop fusion | bytes 16777216 | tf_op jit(solution)/shard_map/squeeze | solution.py:88
  47.1 8.9 %fusion.8 = bf16[512,2048]{1,0:T(8,128)(2,1)S(1)} fusion(bf16[512,2048]{1,0:T(8,128)(2,1)} %all-gather.2.cloned.1.call-done, bf16[2048,512]{1,0:T(8,128)(2,1)} %get-tuple-element.12, bf16[2048,512]{1,0:T(8,128)(2,1)} %get-tuple-element.23, bf16[2048,512]{1,0:T(8,128)(2,1)} %get-tuple-element.11, bf16[2048,512]{1,0:T(8,128)(2,1)} %get-tuple-element.24), kind=kOutput, calls=%fused_computation.8 | convolution fusion | flops 4329570304 | bytes 12582912 | tf_op jit(solution)/shard_map/dot_general | solution.py:90
  62.3 10.4 %pmax.14 = f32[2,512]{1,0:T(2,128)S(1)} all-reduce(f32[2,512]{1,0:T(2,128)S(1)} %get-tuple-element.19), channel_id=1, replica_groups=mesh['grp'=2,'sp'=4,'tp'=4] {'sp'}, use_global_device_ids=true, to_apply=%region_3.5 | all-reduce | flops 1024 | bytes 8192 | tf_op jit(solution)/shard_map/pmax | solution.py:45
  75.5 2.9 convolution_convert_fusion.4
  80.6 12.3 %reduce-scatter.24.cloned.1.call-done = bf16[128,2]{1,0:T(8,128)(2,1)} async-done(((bf16[512,2]{1,0:T(8,128)(2,1)}), bf16[128,2]{1,0:T(8,128)(2,1)}) %reduce-scatter.24.cloned.1.call-update) | async-done | bytes 528
  93.7 21.5 %reduce-scatter.22.cloned.1.call-done = bf16[128,512]{1,0:T(8,128)(2,1)} async-done(((bf16[512,512]{1,0:T(8,128)(2,1)}), bf16[128,512]{1,0:T(8,128)(2,1)}) %reduce-scatter.22.cloned.1.call-update) | async-done | bytes 131088
  119.2 20.0 %reduce-scatter.16.cloned.1.call-done = bf16[32,2048]{1,0:T(8,128)(2,1)} async-done(((bf16[128,2048]{1,0:T(8,128)(2,1)}), bf16[32,2048]{1,0:T(8,128)(2,1)}) %reduce-scatter.16.cloned.1.call-update) | async-done | bytes 131088 | tf_op jit(solution)/shard_map/reduce_scatter | solution.py:60
  141.3 6.6 %all_gather.14 = bf16[128,2048]{1,0:T(8,128)(2,1)S(1)} all-gather(bf16[32,2048]{1,0:T(8,128)(2,1)S(1)} %multiply_convert_fusion.2), channel_id=1, replica_groups=mesh['grp'=2,'sp'=4,'tp'=4] {'tp'}, dimensions={0}, use_global_device_ids=true | all-gather | bytes 655360 | tf_op jit(solution)/shard_map/all_gather | solution.py:27
  152.2 6.0 %collective-permute-done.3 = bf16[128,512]{1,0:T(8,128)(2,1)S(1)} collective-permute-done((bf16[128,512]{1,0:T(8,128)(2,1)S(1)}, bf16[128,512]{1,0:T(8,128)(2,1)S(1)}, u32[]{:S(2)}, u32[]{:S(2)}) %collective-permute-start.3) | collective-permute-done | bytes 131104 | tf_op jit(solution)/shard_map/ppermute | solution.py:36
  158.8 6.9 %collective-permute-done.4 = bf16[128,512]{1,0:T(8,128)(2,1)} collective-permute-done((bf16[128,512]{1,0:T(8,128)(2,1)S(1)}, bf16[128,512]{1,0:T(8,128)(2,1)}, u32[]{:S(2)}, u32[]{:S(2)}) %collective-permute-start.4) | collective-permute-done | bytes 131104 | tf_op jit(solution)/shard_map/ppermute | solution.py:36
  166.7 6.1 %collective-permute-done.5 = bf16[128,512]{1,0:T(8,128)(2,1)} collective-permute-done((bf16[128,512]{1,0:T(8,128)(2,1)}, bf16[128,512]{1,0:T(8,128)(2,1)}, u32[]{:S(2)}, u32[]{:S(2)}) %collective-permute-start.5) | collective-permute-done | bytes 131104 | tf_op jit(solution)/shard_map/ppermute | solution.py:36
  176.0 3.0 multiply_reduce_fusion
  179.1 8.3 %pmax.15 = f32[2,512]{1,0:T(2,128)S(1)} all-reduce(f32[2,512]{1,0:T(2,128)S(1)} %get-tuple-element.21), channel_id=1, replica_groups=mesh['grp'=2,'sp'=4,'tp'=4] {'sp'}, use_global_device_ids=true, to_apply=%region_10.12 | all-reduce | flops 1024 | bytes 8192 | tf_op jit(solution)/shard_map/pmax | solution.py:45
  190.3 2.9 convolution_convert_fusion.3
  195.3 13.8 %reduce-scatter.28.cloned.1.call-done = bf16[128,2]{1,0:T(8,128)(2,1)} async-done(((bf16[512,2]{1,0:T(8,128)(2,1)}), bf16[128,2]{1,0:T(8,128)(2,1)}) %reduce-scatter.28.cloned.1.call-update) | async-done | bytes 528
  209.9 21.3 %reduce-scatter.26.cloned.1.call-done = bf16[128,512]{1,0:T(8,128)(2,1)} async-done(((bf16[512,512]{1,0:T(8,128)(2,1)}), bf16[128,512]{1,0:T(8,128)(2,1)}) %reduce-scatter.26.cloned.1.call-update) | async-done | bytes 131088
  235.3 19.9 %reduce-scatter.18.cloned.1.call-done = bf16[32,2048]{1,0:T(8,128)(2,1)} async-done(((bf16[128,2048]{1,0:T(8,128)(2,1)}), bf16[32,2048]{1,0:T(8,128)(2,1)}) %reduce-scatter.18.cloned.1.call-update) | async-done | bytes 131088 | tf_op jit(solution)/shard_map/reduce_scatter | solution.py:60
  257.3 6.7 %all_gather.15 = bf16[128,2048]{1,0:T(8,128)(2,1)S(1)} all-gather(bf16[32,2048]{1,0:T(8,128)(2,1)S(1)} %multiply_convert_fusion.1), channel_id=1, replica_groups=mesh['grp'=2,'sp'=4,'tp'=4] {'tp'}, dimensions={0}, use_global_device_ids=true | all-gather | bytes 655360 | tf_op jit(solution)/shard_map/all_gather | solution.py:108
  267.9 3.4 %collective-permute-start.6 = (bf16[2,1408]{0,1:T(8,128)(2,1)S(1)}, bf16[2,1408]{0,1:T(8,128)(2,1)S(1)}, u32[]{:S(2)}, u32[]{:S(2)}) collective-permute-start(bf16[2,1408]{0,1:T(8,128)(2,1)S(1)} %pad_maximum_fusion), channel_id=1, source_target_pairs={{0,4},{4,8},{8,12},{1,5},{5,9},{9,13},{2,6},{6,10},{10,14},{3,7},{... | collective-permute-start | bytes 16904 | tf_op jit(solution)/shard_map/ppermute | solution.py:13
  271.5 8.0 %collective-permute-done.6 = bf16[2,1408]{0,1:T(8,128)(2,1)S(1)} collective-permute-done((bf16[2,1408]{0,1:T(8,128)(2,1)S(1)}, bf16[2,1408]{0,1:T(8,128)(2,1)S(1)}, u32[]{:S(2)}, u32[]{:S(2)}) %collective-permute-start.6) | collective-permute-done | bytes 5664 | tf_op jit(solution)/shard_map/ppermute | solution.py:13
  282.4 23.4 %reduce-scatter.20.cloned.1.call-done = bf16[32,2048]{1,0:T(8,128)(2,1)} async-done(((bf16[128,2048]{1,0:T(8,128)(2,1)}), bf16[32,2048]{1,0:T(8,128)(2,1)}) %reduce-scatter.20.cloned.1.call-update) | async-done | bytes 131088 | tf_op jit(solution)/shard_map/reduce_scatter | solution.py:120
  (113 shorter events, 62.6 us)
Async XLA Ops:
  6.5 274.4 %copy-start = (bf16[704,2048]{1,0:T(8,128)(2,1)S(1)}, bf16[704,2048]{1,0:T(8,128)(2,1)}, u32[]{:S(2)}) copy-start(bf16[704,2048]{1,0:T(8,128)(2,1)} %param.30) | copy-start | bytes 8650756
  6.5 40.6 %all-gather.2.cloned.1.call-start = ((), (), s32[]{:S(2)}) async-start(), calls=%async_computation.7 | async-start | bytes 2621440 | tf_op jit(solution)/shard_map/all_gather | solution.py:91
  10.0 82.9 %reduce-scatter.24.cloned.1.call-start = ((), (), s32[]{:S(2)}) async-start(), calls=%async_computation.12 | async-start | bytes 163840
  10.3 26.7 %copy-start.3 = (bf16[2,2048,512]{2,1,0:T(8,128)(2,1)S(1)}, bf16[2,2048,512]{2,1,0:T(8,128)(2,1)}, u32[]{:S(2)}) copy-start(bf16[2,2048,512]{2,1,0:T(8,128)(2,1)} %param.23) | copy-start | bytes 12582916
  22.0 7.6 %collective-permute-start = (bf16[128,512]{1,0:T(8,128)(2,1)S(1)}, bf16[128,512]{1,0:T(8,128)(2,1)S(1)}, u32[]{:S(2)}, u32[]{:S(2)}) collective-permute-start(bf16[128,512]{1,0:T(8,128)(2,1)S(1)} %fusion.25), channel_id=1, source_target_pairs={{0,4},{4,8},{8,12},{12,0},{1,5},{5,9},{9,13},{13,1},{2,6},{6,10},{... | collective-permute-start | bytes 393224 | tf_op jit(solution)/shard_map/ppermute | solution.py:36
  30.2 6.8 %collective-permute-start.1 = (bf16[128,512]{1,0:T(8,128)(2,1)S(1)}, bf16[128,512]{1,0:T(8,128)(2,1)S(1)}, u32[]{:S(2)}, u32[]{:S(2)}) collective-permute-start(bf16[128,512]{1,0:T(8,128)(2,1)S(1)} %collective-permute-done), channel_id=1, source_target_pairs={{0,4},{4,8},{8,12},{12,0},{1,5},{5,9},{9,13},{13,1},{2,6},{6,10},{... | collective-permute-start | bytes 393224 | tf_op jit(solution)/shard_map/ppermute | solution.py:36
  37.0 6.9 %collective-permute-start.2 = (bf16[128,512]{1,0:T(8,128)(2,1)S(1)}, bf16[128,512]{1,0:T(8,128)(2,1)}, u32[]{:S(2)}, u32[]{:S(2)}) collective-permute-start(bf16[128,512]{1,0:T(8,128)(2,1)S(1)} %collective-permute-done.1), channel_id=1, source_target_pairs={{0,4},{4,8},{8,12},{12,0},{1,5},{5,9},{9,13},{13,1},{2,6},{6,10},{... | collective-permute-start | bytes 393224 | tf_op jit(solution)/shard_map/ppermute | solution.py:36
  62.3 13.2 %copy-start.8 = (bf16[512,512]{0,1:T(8,128)(2,1)S(1)}, bf16[512,512]{0,1:T(8,128)(2,1)}, u32[]{:S(2)}) copy-start(bf16[512,512]{0,1:T(8,128)(2,1)} %copy.46) | copy-start | bytes 1572868
  75.5 39.7 %reduce-scatter.22.cloned.1.call-start = ((), (), s32[]{:S(2)}) async-start(), calls=%async_computation.11 | async-start | bytes 655360
  80.5 58.7 %reduce-scatter.16.cloned.1.call-start = ((), (), s32[]{:S(2)}) async-start(), calls=%async_computation.8 | async-start | bytes 655360 | tf_op jit(solution)/shard_map/reduce_scatter | solution.py:60
  119.1 90.0 %reduce-scatter.28.cloned.1.call-start = ((), (), s32[]{:S(2)}) async-start(), calls=%async_computation.14 | async-start | bytes 163840
  140.3 25.4 %copy-start.9 = (bf16[512,512]{1,0:T(8,128)(2,1)S(1)}, bf16[512,512]{1,0:T(8,128)(2,1)}, u32[]{:S(2)}) copy-start(bf16[512,512]{1,0:T(8,128)(2,1)} %get-tuple-element.14) | copy-start | bytes 1572868
  150.6 7.5 %collective-permute-start.3 = (bf16[128,512]{1,0:T(8,128)(2,1)S(1)}, bf16[128,512]{1,0:T(8,128)(2,1)S(1)}, u32[]{:S(2)}, u32[]{:S(2)}) collective-permute-start(bf16[128,512]{1,0:T(8,128)(2,1)S(1)} %fusion.28), channel_id=1, source_target_pairs={{0,4},{4,8},{8,12},{12,0},{1,5},{5,9},{9,13},{13,1},{2,6},{6,10},{... | collective-permute-start | bytes 393224 | tf_op jit(solution)/shard_map/ppermute | solution.py:36
  158.8 6.9 %collective-permute-start.4 = (bf16[128,512]{1,0:T(8,128)(2,1)S(1)}, bf16[128,512]{1,0:T(8,128)(2,1)}, u32[]{:S(2)}, u32[]{:S(2)}) collective-permute-start(bf16[128,512]{1,0:T(8,128)(2,1)S(1)} %collective-permute-done.3), channel_id=1, source_target_pairs={{0,4},{4,8},{8,12},{12,0},{1,5},{5,9},{9,13},{13,1},{2,6},{6,10},{... | collective-permute-start | bytes 393224 | tf_op jit(solution)/shard_map/ppermute | solution.py:36
  165.7 7.1 %collective-permute-start.5 = (bf16[128,512]{1,0:T(8,128)(2,1)}, bf16[128,512]{1,0:T(8,128)(2,1)}, u32[]{:S(2)}, u32[]{:S(2)}) collective-permute-start(bf16[128,512]{1,0:T(8,128)(2,1)} %collective-permute-done.4), channel_id=1, source_target_pairs={{0,4},{4,8},{8,12},{12,0},{1,5},{5,9},{9,13},{13,1},{2,6},{6,10},{... | collective-permute-start | bytes 393224 | tf_op jit(solution)/shard_map/ppermute | solution.py:36
  176.0 14.2 %copy-start.6 = (bf16[512,512]{0,1:T(8,128)(2,1)S(1)}, bf16[512,512]{0,1:T(8,128)(2,1)}, u32[]{:S(2)}) copy-start(bf16[512,512]{0,1:T(8,128)(2,1)} %copy.47) | copy-start | bytes 1572868
  190.2 41.0 %reduce-scatter.26.cloned.1.call-start = ((), (), s32[]{:S(2)}) async-start(), calls=%async_computation.13 | async-start | bytes 655360
  195.2 60.0 %copy-start.2 = (bf16[32,2048]{1,0:T(8,128)(2,1)S(1)}, bf16[32,2048]{1,0:T(8,128)(2,1)}, u32[]{:S(2)}) copy-start(bf16[32,2048]{1,0:T(8,128)(2,1)} %reduce-scatter.16.cloned.1.call-done) | copy-start | bytes 393220
  195.3 59.9 %reduce-scatter.18.cloned.1.call-start = ((), (), s32[]{:S(2)}) async-start(), calls=%async_computation.9 | async-start | bytes 655360 | tf_op jit(solution)/shard_map/reduce_scatter | solution.py:60
  209.9 46.4 %copy-start.18 = (f32[2048]{0:T(1024)S(1)}, f32[2048]{0:T(1024)}, u32[]{:S(2)}) copy-start(f32[2048]{0:T(1024)} %param.25) | copy-start | bytes 24580
  235.2 70.6 %reduce-scatter.20.cloned.1.call-start = ((), (), s32[]{:S(2)}) async-start(), calls=%async_computation.10 | async-start | bytes 655360 | tf_op jit(solution)/shard_map/reduce_scatter | solution.py:120
  267.9 11.6 %collective-permute-start.6 = (bf16[2,1408]{0,1:T(8,128)(2,1)S(1)}, bf16[2,1408]{0,1:T(8,128)(2,1)S(1)}, u32[]{:S(2)}, u32[]{:S(2)}) collective-permute-start(bf16[2,1408]{0,1:T(8,128)(2,1)S(1)} %pad_maximum_fusion), channel_id=1, source_target_pairs={{0,4},{4,8},{8,12},{1,5},{5,9},{9,13},{2,6},{6,10},{10,14},{3,7},{... | collective-permute-start | bytes 16904 | tf_op jit(solution)/shard_map/ppermute | solution.py:13
  280.9 24.9 %copy-start.5 = (bf16[32,2048]{1,0:T(8,128)(2,1)S(1)}, bf16[32,2048]{1,0:T(8,128)(2,1)}, u32[]{:S(2)}) copy-start(bf16[32,2048]{1,0:T(8,128)(2,1)} %reduce-scatter.18.cloned.1.call-done) | copy-start | bytes 393220
  280.9 26.0 %copy-start.19 = (f32[2048]{0:T(1024)S(1)}, f32[2048]{0:T(1024)}, u32[]{:S(2)}) copy-start(f32[2048]{0:T(1024)} %param.31) | copy-start | bytes 24580
  (11 other events, 36.9 us)
Sparse Core Ops, SparseCore 0:
  10.1 25.2 all-gather.1
  75.6 17.2 reduce-scatter.23
  95.2 19.9 reduce-scatter.21
  119.3 19.9 reduce-scatter.15
  190.3 18.7 reduce-scatter.27
  211.2 19.9 reduce-scatter.25
  235.3 19.8 reduce-scatter.17
  282.5 23.2 reduce-scatter.19
